TPU v7x, 32 devices: a whole 2x2x4 slice. The times are simulated.
32 devices in a mesh: fs: 4 (over z), tp: 4 (over y, x), rep: 2 (over core).
Axes of the slice: x: 2, y: 2, z: 4, core: 2. Of those that a mesh axis runs over, the one named last changes fastest.
Arguments:
- up_weight: float32 [2048, 8192], P('fs', ('tp', 'rep')), may hold values from -0.125 to 0.125
- up_momentum: float32 [2048, 8192], P('fs', ('tp', 'rep')), may hold values from -24 to 24
- up_grads: bfloat16 [2, 2048, 8192], P('rep', 'fs', 'tp'), may hold values from -2.09375 to 2.09375
- out_weight: float32 [2048, 2048], P('fs', ('tp', 'rep')), may hold values from -0.125 to 0.125
- out_momentum: float32 [2048, 2048], P('fs', ('tp', 'rep')), may hold values from -24 to 24
- out_grads: bfloat16 [2, 2048, 2048], P('rep', 'fs', 'tp'), may hold values from -2.09375 to 2.09375
Outputs:
- up_weight_new: float32 [2048, 8192], P('fs', ('tp', 'rep'))
- up_momentum_new: float32 [2048, 8192], P('fs', ('tp', 'rep'))
- up_direction: float32 [2048, 8192], P('fs', ('tp', 'rep'))
- out_weight_new: float32 [2048, 2048], P('fs', ('tp', 'rep'))
- out_momentum_new: float32 [2048, 2048], P('fs', ('tp', 'rep'))
- out_direction: float32 [2048, 2048], P('fs', ('tp', 'rep'))
All inputs are finite; a program needn't handle non-finite values.
Results may differ from a plain program's by a relative error of at most 0.039.
Values may be sent and summed in bfloat16 or wider, within the bound.
No kernel may reach another device: no remote copies, remote signals or barrier semaphores. Data moves between devices by JAX's collectives and lax.ppermute only.
A program may use at most 64 MiB of HBM per device.

v0:
```python
import math

import jax
import jax.numpy as jnp
from jax import lax
from jax.sharding import PartitionSpec as P

ITERS = 3


MOMENT = 0.9
RATE = 0.02
COEF_A = 3.4445
COEF_B = -4.775
COEF_C = 2.0315


def local_gram(values, columns):
    return lax.dot_general(
        values, columns, (((1,), (1,)), ((), ())), preferred_element_type=jnp.float32
    )


def contract(gram, values, gram_axis):
    return lax.dot_general(
        gram, values, (((gram_axis,), (0,)), ((), ())), preferred_element_type=jnp.float32
    )


def second_product(gram, first_half, gram_axis):
    return contract(gram, lax.all_gather(first_half, "fs", axis=0, tiled=True), gram_axis)


def on_device(up_weight, up_momentum, up_grads, out_weight, out_momentum, out_grads):
    grad_up, grad_out = (
        lax.psum_scatter(
            up_grads[0].astype(jnp.float32).astype(jnp.bfloat16),
            "rep",
            scatter_dimension=1,
            tiled=True,
        ).astype(jnp.float32),
        lax.psum_scatter(
            out_grads[0].astype(jnp.float32).astype(jnp.bfloat16),
            "rep",
            scatter_dimension=1,
            tiled=True,
        ).astype(jnp.float32),
    )
    moments = [MOMENT * up_momentum + grad_up, MOMENT * out_momentum + grad_out]
    group = lax.axis_size("tp") * lax.axis_size("rep")
    current = moments
    for iteration in range(ITERS):
        values = [entry.astype(jnp.bfloat16) for entry in current]
        columns = (
            lax.all_gather(values[0], "fs", axis=0, tiled=True),
            lax.all_gather(values[1], "fs", axis=0, tiled=True),
        )
        gram_sums = (
            lax.psum(local_gram(values[0], columns[0]).astype(jnp.bfloat16), ("tp", "rep")).astype(
                jnp.float32
            ),
            lax.psum(local_gram(values[1], columns[1]).astype(jnp.bfloat16), ("tp", "rep")).astype(
                jnp.float32
            ),
        )
        gram_axis = 1
        if iteration == 0:
            totals = lax.psum(
                (jnp.sum(gram_sums[0] * gram_sums[0]), jnp.sum(gram_sums[1] * gram_sums[1])), "fs"
            )
        if iteration == 0:
            squares = [1.0 / (jnp.sqrt(total) + 1.0) for total in totals]
            factors = [jnp.sqrt(square) for square in squares]
        else:
            squares = [1.0, 1.0]
            factors = [1.0, 1.0]
        halves = [(gram_sums[index] * squares[index]).astype(jnp.bfloat16) for index in range(2)]
        products = [
            factors[index] * contract(halves[index], columns[index], gram_axis)
            for index in range(2)
        ]
        seconds = [
            second_product(halves[index], products[index].astype(jnp.bfloat16), gram_axis)
            for index in range(2)
        ]
        current = [
            COEF_A * factors[index] * current[index]
            + COEF_B * products[index]
            + COEF_C * seconds[index]
            for index in range(2)
        ]
    widths = [up_weight.shape[1] * group, out_weight.shape[1] * group]
    directions = [current[index] * math.sqrt(widths[index]) for index in range(2)]
    return (
        up_weight - RATE * directions[0],
        moments[0],
        directions[0],
        out_weight - RATE * directions[1],
        moments[1],
        directions[1],
    )


def solution(mesh):
    return jax.shard_map(
        on_device,
        mesh=mesh,
        in_specs=(
            P("fs", ("tp", "rep")),
            P("fs", ("tp", "rep")),
            P("rep", "fs", "tp"),
            P("fs", ("tp", "rep")),
            P("fs", ("tp", "rep")),
            P("rep", "fs", "tp"),
        ),
        out_specs=(
            P("fs", ("tp", "rep")),
            P("fs", ("tp", "rep")),
            P("fs", ("tp", "rep")),
            P("fs", ("tp", "rep")),
            P("fs", ("tp", "rep")),
            P("fs", ("tp", "rep")),
        ),
        check_vma=False,
    )
```

profile of v0, /device:TPU:0, one launch (start us, length us, event | category | flops | bytes accessed | tf_op | source)
XLA Modules:
  0.0 994.7 jit_solution(5314064352922162735)
XLA Ops:
  7.2 0.7 reduce-scatter.5.cloned.1.call-update
  8.0 0.7 reduce-scatter.3.cloned.1.call-update
  8.7 12.2 %reduce-scatter.5.cloned.1.call-done = bf16[512,256]{1,0:T(8,128)(2,1)} async-done(((bf16[512,512]{1,0:T(8,128)(2,1)}), bf16[512,256]{1,0:T(8,128)(2,1)}) %reduce-scatter.5.cloned.1.call-update) | async-done | bytes 262160 | tf_op jit(solution)/shard_map/reduce_scatter | solution.py:42
  20.9 1.9 fusion.25
  22.9 11.0 %reduce-scatter.3.cloned.1.call-done = bf16[512,1024]{1,0:T(8,128)(2,1)} async-done(((bf16[512,2048]{1,0:T(8,128)(2,1)}), bf16[512,1024]{1,0:T(8,128)(2,1)}) %reduce-scatter.3.cloned.1.call-update) | async-done | bytes 1048592 | tf_op jit(solution)/shard_map/reduce_scatter | solution.py:36
  33.9 3.3 fusion.26
  37.3 0.0 all-reduce.12.cloned.1.call-start
  37.3 28.1 %all-gather.25.cloned.1.call-done = bf16[2048,256]{1,0:T(8,128)(2,1)} async-done(((bf16[512,256]{1,0:T(8,128)(2,1)}), bf16[2048,256]{1,0:T(8,128)(2,1)}) %all-gather.25.cloned.1.call-update) | async-done | bytes 1048592 | tf_op jit(solution)/shard_map/all_gather | solution.py:56
  65.4 3.3 convolution_convert_fusion.2
  68.7 78.9 %all-gather.13.cloned.1.call-done = bf16[2048,1024]{1,0:T(8,128)(2,1)} async-done(((bf16[512,1024]{1,0:T(8,128)(2,1)}), bf16[2048,1024]{1,0:T(8,128)(2,1)}) %all-gather.13.cloned.1.call-update) | async-done | bytes 4194320 | tf_op jit(solution)/shard_map/all_gather | solution.py:55
  147.5 5.9 convolution_convert_fusion.5
  153.5 79.4 %all-reduce.12.cloned.1.call-done = (bf16[512,2048]{1,0:T(8,128)(2,1)}, bf16[512,2048]{1,0:T(8,128)(2,1)}) async-done(((bf16[512,2048]{1,0:T(8,128)(2,1)}, bf16[512,2048]{1,0:T(8,128)(2,1)}), (bf16[512,2048]{1,0:T(8,128)(2,1)}, bf16[512,2048]{1,0:T(8,128)(2,1)})) %all-reduce.12.cloned.1.call-update) | async-done | bytes 4194320 | tf_op jit(solution)/shard_map/psum | solution.py:59
  232.9 4.0 fusion
  236.9 12.3 %all-reduce = (f32[]{:T(128)}, f32[]{:T(128)}) all-reduce(f32[]{:T(128)} %get-tuple-element.42, f32[]{:T(128)} %get-tuple-element.43), channel_id=1, replica_groups=mesh['fs'=4,'tp'=4,'rep'=2] {'fs'}, use_global_device_ids=true, to_apply=%region_3.0 | all-reduce | flops 2 | bytes 16 | tf_op jit(solution)/shard_map/psum | solution.py:68
  250.0 3.3 fusion.28
  254.2 6.3 multiply_convert_fusion
  260.5 0.0 all-gather.29.cloned.1.call-start
  260.6 18.3 %all-gather.27.cloned.1.call-done = bf16[2048,256]{1,0:T(8,128)(2,1)} async-done(((bf16[512,256]{1,0:T(8,128)(2,1)}), bf16[2048,256]{1,0:T(8,128)(2,1)}) %all-gather.27.cloned.1.call-update) | async-done | bytes 1048592 | tf_op jit(solution)/shard_map/all_gather | solution.py:31
  278.8 3.6 fusion.29
  282.5 78.6 %all-gather.15.cloned.1.call-done = bf16[2048,1024]{1,0:T(8,128)(2,1)} async-done(((bf16[512,1024]{1,0:T(8,128)(2,1)}), bf16[2048,1024]{1,0:T(8,128)(2,1)}) %all-gather.15.cloned.1.call-update) | async-done | bytes 4194320 | tf_op jit(solution)/shard_map/all_gather | solution.py:31
  361.1 7.6 fusion.27
  368.7 0.2 all-reduce.10.cloned.1.call-start
  369.0 20.8 %all-gather.29.cloned.1.call-done = bf16[2048,256]{1,0:T(8,128)(2,1)} async-done(((bf16[512,256]{1,0:T(8,128)(2,1)}), bf16[2048,256]{1,0:T(8,128)(2,1)}) %all-gather.29.cloned.1.call-update) | async-done | bytes 1048592 | tf_op jit(solution)/shard_map/all_gather | solution.py:56
  389.8 3.3 convolution_convert_fusion.1
  393.1 79.0 %all-gather.17.cloned.1.call-done = bf16[2048,1024]{1,0:T(8,128)(2,1)} async-done(((bf16[512,1024]{1,0:T(8,128)(2,1)}), bf16[2048,1024]{1,0:T(8,128)(2,1)}) %all-gather.17.cloned.1.call-update) | async-done | bytes 4194320 | tf_op jit(solution)/shard_map/all_gather | solution.py:55
  472.1 5.9 convolution_convert_fusion.4
  478.0 0.0 all-gather.31.cloned.1.call-start
  478.0 79.4 %all-reduce.10.cloned.1.call-done = (bf16[512,2048]{1,0:T(8,128)(2,1)}, bf16[512,2048]{1,0:T(8,128)(2,1)}) async-done(((bf16[512,2048]{1,0:T(8,128)(2,1)}, bf16[512,2048]{1,0:T(8,128)(2,1)}), (bf16[512,2048]{1,0:T(8,128)(2,1)}, bf16[512,2048]{1,0:T(8,128)(2,1)})) %all-reduce.10.cloned.1.call-update) | async-done | bytes 4194320 | tf_op jit(solution)/shard_map/psum | solution.py:59
  557.5 3.0 fusion.32
  560.5 0.0 all-gather.19.cloned.1.call-start
  560.6 6.9 fusion.30
  567.5 0.0 all-gather.33.cloned.1.call-start
  567.6 21.1 %all-gather.31.cloned.1.call-done = bf16[2048,256]{1,0:T(8,128)(2,1)} async-done(((bf16[512,256]{1,0:T(8,128)(2,1)}), bf16[2048,256]{1,0:T(8,128)(2,1)}) %all-gather.31.cloned.1.call-update) | async-done | bytes 1048592 | tf_op jit(solution)/shard_map/all_gather | solution.py:31
  588.7 2.8 fusion.33
  591.6 78.7 %all-gather.19.cloned.1.call-done = bf16[2048,1024]{1,0:T(8,128)(2,1)} async-done(((bf16[512,1024]{1,0:T(8,128)(2,1)}), bf16[2048,1024]{1,0:T(8,128)(2,1)}) %all-gather.19.cloned.1.call-update) | async-done | bytes 4194320 | tf_op jit(solution)/shard_map/all_gather | solution.py:31
  670.3 8.4 fusion.31
  678.7 20.2 %all-gather.33.cloned.1.call-done = bf16[2048,256]{1,0:T(8,128)(2,1)} async-done(((bf16[512,256]{1,0:T(8,128)(2,1)}), bf16[2048,256]{1,0:T(8,128)(2,1)}) %all-gather.33.cloned.1.call-update) | async-done | bytes 1048592 | tf_op jit(solution)/shard_map/all_gather | solution.py:56
  698.9 3.3 convolution_convert_fusion
  702.2 78.3 %all-gather.21.cloned.1.call-done = bf16[2048,1024]{1,0:T(8,128)(2,1)} async-done(((bf16[512,1024]{1,0:T(8,128)(2,1)}), bf16[2048,1024]{1,0:T(8,128)(2,1)}) %all-gather.21.cloned.1.call-update) | async-done | bytes 4194320 | tf_op jit(solution)/shard_map/all_gather | solution.py:55
  780.5 5.9 convolution_convert_fusion.3
  786.4 79.4 %all-reduce.8.cloned.1.call-done = (bf16[512,2048]{1,0:T(8,128)(2,1)}, bf16[512,2048]{1,0:T(8,128)(2,1)}) async-done(((bf16[512,2048]{1,0:T(8,128)(2,1)}, bf16[512,2048]{1,0:T(8,128)(2,1)}), (bf16[512,2048]{1,0:T(8,128)(2,1)}, bf16[512,2048]{1,0:T(8,128)(2,1)})) %all-reduce.8.cloned.1.call-update) | async-done | bytes 4194320 | tf_op jit(solution)/shard_map/psum | solution.py:59
  865.9 3.0 fusion.35
  868.9 0.3 all-gather.23.cloned.1.call-start
  869.2 7.0 fusion.34
  876.2 20.9 %all-gather.35.cloned.1.call-done = bf16[2048,256]{1,0:T(8,128)(2,1)} async-done(((bf16[512,256]{1,0:T(8,128)(2,1)}), bf16[2048,256]{1,0:T(8,128)(2,1)}) %all-gather.35.cloned.1.call-update) | async-done | bytes 1048592 | tf_op jit(solution)/shard_map/all_gather | solution.py:31
  897.1 3.1 broadcast_multiply_fusion.1
  900.2 78.5 %all-gather.23.cloned.1.call-done = bf16[2048,1024]{1,0:T(8,128)(2,1)} async-done(((bf16[512,1024]{1,0:T(8,128)(2,1)}), bf16[2048,1024]{1,0:T(8,128)(2,1)}) %all-gather.23.cloned.1.call-update) | async-done | bytes 4194320 | tf_op jit(solution)/shard_map/all_gather | solution.py:31
  978.7 9.5 broadcast_multiply_fusion
  (59 shorter events, 0.7 us)
Async XLA Ops:
  7.2 13.7 %copy-start.14 = (f32[512,256]{1,0:T(8,128)S(1)}, f32[512,256]{1,0:T(8,128)}, u32[]{:S(2)}) copy-start(f32[512,256]{1,0:T(8,128)} %param.10) | copy-start | bytes 1572868
  7.2 13.7 %reduce-scatter.5.cloned.1.call-start = ((), (), s32[]{:S(2)}) async-start(), calls=%async_computation.9 | async-start | bytes 786432 | tf_op jit(solution)/shard_map/reduce_scatter | solution.py:42
  7.9 26.0 %copy-start.7 = (f32[512,1024]{1,0:T(8,128)S(1)}, f32[512,1024]{1,0:T(8,128)}, u32[]{:S(2)}) copy-start(f32[512,1024]{1,0:T(8,128)} %param.7) | copy-start | bytes 6291460
  7.9 26.0 %reduce-scatter.3.cloned.1.call-start = ((), (), s32[]{:S(2)}) async-start(), calls=%async_computation.2 | async-start | bytes 3145728 | tf_op jit(solution)/shard_map/reduce_scatter | solution.py:36
  8.7 56.7 %all-gather.25.cloned.1.call-start = ((), (), s32[]{:S(2)}) async-start(), calls=%async_computation.10 | async-start | bytes 1310720 | tf_op jit(solution)/shard_map/all_gather | solution.py:56
  22.8 42.6 %copy-start.6 = (bf16[512,256]{1,0:T(8,128)(2,1)S(1)}, bf16[512,256]{1,0:T(8,128)(2,1)}, u32[]{:S(2)}) copy-start(bf16[512,256]{1,0:T(8,128)(2,1)} %get-tuple-element.14) | copy-start | bytes 786436
  22.8 124.7 %all-gather.13.cloned.1.call-start = ((), (), s32[]{:S(2)}) async-start(), calls=%async_computation.3 | async-start | bytes 5242880 | tf_op jit(solution)/shard_map/all_gather | solution.py:55
  37.2 110.3 %copy-start.4 = (bf16[512,1024]{1,0:T(8,128)(2,1)S(1)}, bf16[512,1024]{1,0:T(8,128)(2,1)}, u32[]{:S(2)}) copy-start(bf16[512,1024]{1,0:T(8,128)(2,1)} %get-tuple-element.16) | copy-start | bytes 3145732
  37.3 195.7 %all-reduce.12.cloned.1.call-start = ((), (), s32[]{:S(2)}) async-start(), calls=%async_computation.18 | async-start | bytes 8388608 | tf_op jit(solution)/shard_map/psum | solution.py:59
  153.4 125.4 %all-gather.27.cloned.1.call-start = ((), (), s32[]{:S(2)}) async-start(), calls=%async_computation.11 | async-start | bytes 1310720 | tf_op jit(solution)/shard_map/all_gather | solution.py:31
  232.9 17.1 %copy-start.10 = (bf16[2048,256]{1,0:T(8,128)(2,1)S(1)}, bf16[2048,256]{1,0:T(8,128)(2,1)}, u32[]{:S(2)}) copy-start(bf16[2048,256]{1,0:T(8,128)(2,1)} %all-gather.25.cloned.1.call-done) | copy-start | bytes 3145732
  250.0 4.2 copy-start.9
  253.4 107.8 %all-gather.15.cloned.1.call-start = ((), (), s32[]{:S(2)}) async-start(), calls=%async_computation.4 | async-start | bytes 5242880 | tf_op jit(solution)/shard_map/all_gather | solution.py:31
  254.2 24.7 %copy-start.15 = (f32[512,256]{1,0:T(8,128)S(1)}, f32[512,256]{1,0:T(8,128)}, u32[]{:S(2)}) copy-start(f32[512,256]{1,0:T(8,128)} %get-tuple-element.15) | copy-start | bytes 1572868
  254.2 24.6 %copy-start.16 = (f32[512,256]{1,0:T(8,128)S(1)}, f32[512,256]{1,0:T(8,128)}, u32[]{:S(2)}) copy-start(f32[512,256]{1,0:T(8,128)} %get-tuple-element.27) | copy-start | bytes 1572868
  260.5 129.3 %all-gather.29.cloned.1.call-start = ((), (), s32[]{:S(2)}) async-start(), calls=%async_computation.12 | async-start | bytes 1310720 | tf_op jit(solution)/shard_map/all_gather | solution.py:56
  278.8 82.3 %copy-start.8 = (f32[512,1024]{1,0:T(8,128)S(1)}, f32[512,1024]{1,0:T(8,128)}, u32[]{:S(2)}) copy-start(f32[512,1024]{1,0:T(8,128)} %get-tuple-element.17) | copy-start | bytes 6291460
  282.5 189.6 %all-gather.17.cloned.1.call-start = ((), (), s32[]{:S(2)}) async-start(), calls=%async_computation.5 | async-start | bytes 5242880 | tf_op jit(solution)/shard_map/all_gather | solution.py:55
  361.1 28.6 %copy-start.13 = (bf16[512,256]{1,0:T(8,128)(2,1)S(1)}, bf16[512,256]{1,0:T(8,128)(2,1)}, u32[]{:S(2)}) copy-start(bf16[512,256]{1,0:T(8,128)(2,1)} %get-tuple-element.28) | copy-start | bytes 786436
  368.7 103.4 %copy-start.11 = (bf16[512,1024]{1,0:T(8,128)(2,1)S(1)}, bf16[512,1024]{1,0:T(8,128)(2,1)}, u32[]{:S(2)}) copy-start(bf16[512,1024]{1,0:T(8,128)(2,1)} %get-tuple-element.24) | copy-start | bytes 3145732
  368.7 188.7 %all-reduce.10.cloned.1.call-start = ((), (), s32[]{:S(2)}) async-start(), calls=%async_computation.17 | async-start | bytes 8388608 | tf_op jit(solution)/shard_map/psum | solution.py:59
  477.9 79.5 %copy-start.2 = (bf16[2048,256]{1,0:T(8,128)(2,1)S(1)}, bf16[2048,256]{1,0:T(8,128)(2,1)}, u32[]{:S(2)}) copy-start(bf16[2048,256]{1,0:T(8,128)(2,1)} %all-gather.29.cloned.1.call-done) | copy-start | bytes 3145732
  478.0 110.7 %all-gather.31.cloned.1.call-start = ((), (), s32[]{:S(2)}) async-start(), calls=%async_computation.13 | async-start | bytes 1310720 | tf_op jit(solution)/shard_map/all_gather | solution.py:31
  560.5 109.8 %all-gather.19.cloned.1.call-start = ((), (), s32[]{:S(2)}) async-start(), calls=%async_computation.6 | async-start | bytes 5242880 | tf_op jit(solution)/shard_map/all_gather | solution.py:31
  560.5 28.2 %copy-start = (bf16[512,2048]{1,0:T(8,128)(2,1)S(1)}, bf16[512,2048]{1,0:T(8,128)(2,1)}, u32[]{:S(2)}) copy-start(bf16[512,2048]{1,0:T(8,128)(2,1)} %get-tuple-element.11) | copy-start | bytes 6291460
  567.5 131.4 %all-gather.33.cloned.1.call-start = ((), (), s32[]{:S(2)}) async-start(), calls=%async_computation.14 | async-start | bytes 1310720 | tf_op jit(solution)/shard_map/all_gather | solution.py:56
  591.5 189.0 %all-gather.21.cloned.1.call-start = ((), (), s32[]{:S(2)}) async-start(), calls=%async_computation.7 | async-start | bytes 5242880 | tf_op jit(solution)/shard_map/all_gather | solution.py:55
  670.3 28.6 %copy-start.5 = (bf16[512,256]{1,0:T(8,128)(2,1)S(1)}, bf16[512,256]{1,0:T(8,128)(2,1)}, u32[]{:S(2)}) copy-start(bf16[512,256]{1,0:T(8,128)(2,1)} %get-tuple-element.36) | copy-start | bytes 786436
  678.6 101.9 %copy-start.12 = (bf16[512,1024]{1,0:T(8,128)(2,1)S(1)}, bf16[512,1024]{1,0:T(8,128)(2,1)}, u32[]{:S(2)}) copy-start(bf16[512,1024]{1,0:T(8,128)(2,1)} %get-tuple-element.32) | copy-start | bytes 3145732
  678.6 187.2 %all-reduce.8.cloned.1.call-start = ((), (), s32[]{:S(2)}) async-start(), calls=%async_computation.16 | async-start | bytes 8388608 | tf_op jit(solution)/shard_map/psum | solution.py:59
  786.4 79.5 %copy-start.3 = (bf16[2048,256]{1,0:T(8,128)(2,1)S(1)}, bf16[2048,256]{1,0:T(8,128)(2,1)}, u32[]{:S(2)}) copy-start(bf16[2048,256]{1,0:T(8,128)(2,1)} %all-gather.33.cloned.1.call-done) | copy-start | bytes 3145732
  786.4 110.7 %all-gather.35.cloned.1.call-start = ((), (), s32[]{:S(2)}) async-start(), calls=%async_computation.15 | async-start | bytes 1310720 | tf_op jit(solution)/shard_map/all_gather | solution.py:31
  868.9 109.8 %all-gather.23.cloned.1.call-start = ((), (), s32[]{:S(2)}) async-start(), calls=%async_computation.8 | async-start | bytes 5242880 | tf_op jit(solution)/shard_map/all_gather | solution.py:31
  869.2 27.9 %copy-start.1 = (bf16[512,2048]{1,0:T(8,128)(2,1)S(1)}, bf16[512,2048]{1,0:T(8,128)(2,1)}, u32[]{:S(2)}) copy-start(bf16[512,2048]{1,0:T(8,128)(2,1)} %get-tuple-element.9) | copy-start | bytes 6291460
Sparse Core Ops, SparseCore 0:
  10.2 10.6 reduce-scatter.4
  23.1 10.7 reduce-scatter.2
  36.1 29.2 all-gather.24
  67.4 80.1 all-gather.12
  153.5 79.3 all-reduce.11
  253.5 25.3 all-gather.26
  281.0 80.1 all-gather.14
  363.3 26.4 all-gather.28
  391.9 80.1 all-gather.16
  478.1 79.3 all-reduce.9
  560.6 28.0 all-gather.30
  590.1 80.1 all-gather.18
  672.4 26.4 all-gather.32
  700.3 80.0 all-gather.20
  786.5 79.3 all-reduce.7
  869.0 28.0 all-gather.34
  898.5 80.1 all-gather.22
where the time goes:
time: 995 us
  waiting for transfers between devices  864 us (87%)
  matrix products  91.9 us (9%)
  between operations  15.6 us (2%)
  blocking collectives  12.3 us (1%)
    all_gather x6, waiting for transfers between devices, second_product(): lax.all_gather(first_half, 'fs', axis=0, tiled=True)  296 us
    psum x3, waiting for transfers between devices, on_device(): lax.psum(local_gram(values[0], columns[0]).astype(jnp.bfloat16), ('tp', '...  238 us
    all_gather x3, waiting for transfers between devices, on_device(): lax.all_gather(values[0], 'fs', axis=0, tiled=True)  236 us
    all_gather x3, waiting for transfers between devices, on_device(): lax.all_gather(values[1], 'fs', axis=0, tiled=True)  69.1 us
    dot_general x12, matrix products, contract(): lax.dot_general(gram, values, (((gram_axis,), (0,)), ((), ())), preferred...  64.4 us
    dot_general x6, matrix products, local_gram(): lax.dot_general(values, columns, (((1,), (1,)), ((), ())), preferred_elem...  27.5 us
  transfers between devices with their start and end apart: 17, of which 17 were waited for; matrix products, arithmetic and copies ran while one was open for 6% of the time, Pallas kernels for 0%

commit v1 on v0

v1 whole, which is shorter than its diff:
```python
import math

import jax
import jax.numpy as jnp
from jax import lax
from jax.sharding import PartitionSpec as P

ITERS = 3


MOMENT = 0.9
RATE = 0.02
COEF_A = 3.4445
COEF_B = -4.775
COEF_C = 2.0315


def rows_times(rows, matrix):
    return lax.dot_general(
        rows.astype(jnp.bfloat16),
        matrix,
        (((1,), (0,)), ((), ())),
        preferred_element_type=jnp.float32,
    )


def local_gram(values, columns):
    return lax.dot_general(
        values, columns, (((1,), (1,)), ((), ())), preferred_element_type=jnp.float32
    )


def reduce_grads(grads):
    return lax.psum_scatter(grads[0], "rep", scatter_dimension=1, tiled=True).astype(jnp.float32)


def on_device(up_weight, up_momentum, up_grads, out_weight, out_momentum, out_grads):
    n_rep, n_tp = lax.axis_size("rep"), lax.axis_size("tp")
    group = n_tp * n_rep
    moments = [
        MOMENT * up_momentum + reduce_grads(up_grads),
        MOMENT * out_momentum + reduce_grads(out_grads),
    ]
    values = [entry.astype(jnp.bfloat16) for entry in moments]
    columns = [lax.all_gather(entry, "fs", axis=0, tiled=True) for entry in values]
    partial = jnp.concatenate(
        [local_gram(values[k], columns[k]).astype(jnp.bfloat16) for k in range(2)], axis=0
    )
    mine = lax.psum_scatter(partial, ("rep", "tp"), scatter_dimension=0, tiled=True)
    block = mine.shape[0]
    shard = values[0].shape[0]
    size = mine.shape[1]
    half = n_rep // 2
    rep = lax.axis_index("rep")
    if half == 1:
        gram = lax.all_gather(mine, ("fs", "tp"), axis=0, tiled=True)
    else:
        both = lax.all_gather(mine, ("fs", "rep", "tp"), axis=0, tiled=True)
        both = both.reshape(-1, 2, shard, size)
        gram = lax.dynamic_index_in_dim(both, rep // half, 1, keepdims=False).reshape(size, size)
    first = lax.axis_index("fs") * shard + ((rep % half) * n_tp + lax.axis_index("tp")) * block
    wide = gram.astype(jnp.float32)
    square = 1.0 / (jnp.sqrt(jnp.sum(wide * wide)) + 1.0)
    factor = jnp.sqrt(square)

    step0 = (
        COEF_B * square * wide + (COEF_C * square * square) * rows_times(gram, gram)
    ).astype(jnp.bfloat16)
    turned = ((COEF_A * square) * wide + square * rows_times(step0, gram)).astype(jnp.bfloat16)
    gram1 = (COEF_A * turned.astype(jnp.float32) + rows_times(turned, step0)).astype(jnp.bfloat16)

    def apply1(rows):
        once = rows_times(rows, gram1)
        return COEF_A * rows + COEF_B * once + COEF_C * rows_times(once, gram1)

    step0_rows = lax.dynamic_slice_in_dim(step0, first, block, 0).astype(jnp.float32)
    gram1_rows = lax.dynamic_slice_in_dim(gram1, first, block, 0).astype(jnp.float32)
    step1_rows = COEF_B * gram1_rows + COEF_C * rows_times(gram1_rows, gram1)
    gram2_rows = apply1(COEF_A * gram1_rows + rows_times(step1_rows, gram1))
    gram2_square = apply1(rows_times(apply1(gram2_rows), gram1))
    step2_rows = COEF_B * gram2_rows + COEF_C * gram2_square
    joined = COEF_A * step1_rows + apply1(step2_rows)
    total = COEF_A * COEF_A * step0_rows + COEF_A * joined + rows_times(joined, step0)
    row_ids = first + lax.broadcasted_iota(jnp.int32, total.shape, 0)
    column_ids = lax.broadcasted_iota(jnp.int32, total.shape, 1)
    total = factor * (total + jnp.where(row_ids == column_ids, COEF_A**ITERS, 0.0))
    maps = lax.all_gather(total.astype(jnp.bfloat16), ("rep", "tp"), axis=0, tiled=True)

    widths = [up_weight.shape[1] * group, out_weight.shape[1] * group]
    directions = [
        math.sqrt(widths[k]) * rows_times(maps[k * shard : (k + 1) * shard], columns[k])
        for k in range(2)
    ]
    return (
        up_weight - RATE * directions[0],
        moments[0],
        directions[0],
        out_weight - RATE * directions[1],
        moments[1],
        directions[1],
    )


def solution(mesh):
    return jax.shard_map(
        on_device,
        mesh=mesh,
        in_specs=(
            P("fs", ("tp", "rep")),
            P("fs", ("tp", "rep")),
            P("rep", "fs", "tp"),
            P("fs", ("tp", "rep")),
            P("fs", ("tp", "rep")),
            P("rep", "fs", "tp"),
        ),
        out_specs=(
            P("fs", ("tp", "rep")),
            P("fs", ("tp", "rep")),
            P("fs", ("tp", "rep")),
            P("fs", ("tp", "rep")),
            P("fs", ("tp", "rep")),
            P("fs", ("tp", "rep")),
        ),
        check_vma=False,
    )
```

time: 995 us -> 484 us (0.49)
  waiting for transfers between devices: 864 us -> 331 us
  matrix products: 91.9 us -> 113 us
  blocking collectives: 12.3 us -> 0 us
    all_gather x12 -> x4, waiting for transfers between devices: 601 us -> 257 us  [the longest x1 114 us: on_device(): gram = lax.all_gather(mine, ('fs', 'tp'), axis=0, tiled=True)]
    psum x3 -> x0, waiting for transfers between devices: 238 us -> none  [on_device(): lax.psum(local_gram(values[0], columns[0]).astype(jnp.bfloat16), ('tp', '...]
    reduce_scatter x2 -> x3, waiting for transfers between devices: 23.2 us -> 72.8 us  [the longest x1 49.8 us: on_device(): lax.psum_scatter(partial, ('rep', 'tp'), scatter_dimension=0, tiled=True)]
    dot_general x12 -> x16, matrix products: 64.4 us -> 106 us  [rows_times(): lax.dot_general(rows.astype(jnp.bfloat16), matrix, (((1,), (0,)), ((), ()...]
    dot_general x6 -> x2, matrix products: 27.5 us -> 6.93 us  [local_gram(): lax.dot_general(values, columns, (((1,), (1,)), ((), ())), preferred_elem...]
    psum x1 -> x0, blocking collectives: 12.3 us -> none  [on_device(): lax.psum((jnp.sum(gram_sums[0] * gram_sums[0]), jnp.sum(gram_sums[1] * gr...]
  transfers between devices with their start and end apart: 17 -> 7, of which waited for: 17 -> 7; matrix products, arithmetic and copies ran while one was open for 6% -> 2% of each run, Pallas kernels for 0% -> 0%
where the time goes in v1:
time: 484 us; the launch traced here: 478 us
  waiting for transfers between devices  331 us (68%)
  matrix products  113 us (23%)
  other arithmetic  17.5 us (4%)
  between operations  15.3 us (3%)
    all_gather x1, waiting for transfers between devices, on_device(): gram = lax.all_gather(mine, ('fs', 'tp'), axis=0, tiled=True)  114 us
    all_gather x2, waiting for transfers between devices, on_device(): lax.all_gather(entry, 'fs', axis=0, tiled=True)  107 us
    dot_general x16, matrix products, rows_times(): lax.dot_general(rows.astype(jnp.bfloat16), matrix, (((1,), (0,)), ((), ()...  106 us
    reduce_scatter x1, waiting for transfers between devices, on_device(): lax.psum_scatter(partial, ('rep', 'tp'), scatter_dimension=0, tiled=True)  49.8 us
    all_gather x1, waiting for transfers between devices, on_device(): lax.all_gather(total.astype(jnp.bfloat16), ('rep', 'tp'), axis=0, tiled=T...  34.9 us
    reduce_scatter x2, waiting for transfers between devices, reduce_grads(): lax.psum_scatter(grads[0], 'rep', scatter_dimension=1, tiled=True)  23.1 us
  transfers between devices with their start and end apart: 7, of which 7 were waited for; matrix products, arithmetic and copies ran while one was open for 2% of the time, Pallas kernels for 0%

profile of v1, /device:TPU:0, one launch (start us, length us, event | category | flops | bytes accessed | tf_op | source)
XLA Modules:
  0.0 478.3 jit_solution(12128783414956549829)
XLA Ops:
  7.2 0.0 reduce-scatter.6.cloned.1.call-start
  7.2 0.7 reduce-scatter.6.cloned.1.call-update
  7.9 0.0 reduce-scatter.4.cloned.1.call-start
  7.9 0.7 reduce-scatter.4.cloned.1.call-update
  8.7 0.0 all-gather.7.cloned.1.call-start
  8.7 12.2 %reduce-scatter.6.cloned.1.call-done = bf16[512,256]{1,0:T(8,128)(2,1)} async-done(((bf16[512,512]{1,0:T(8,128)(2,1)}), bf16[512,256]{1,0:T(8,128)(2,1)}) %reduce-scatter.6.cloned.1.call-update) | async-done | bytes 262160 | tf_op jit(solution)/shard_map/reduce_scatter | solution.py:34
  20.9 2.1 fusion.45
  23.0 0.0 all-gather.7.cloned.1.call-update
  23.0 0.0 all-gather.5.cloned.1.call-start
  23.0 10.9 %reduce-scatter.4.cloned.1.call-done = bf16[512,1024]{1,0:T(8,128)(2,1)} async-done(((bf16[512,2048]{1,0:T(8,128)(2,1)}), bf16[512,1024]{1,0:T(8,128)(2,1)}) %reduce-scatter.4.cloned.1.call-update) | async-done | bytes 1048592 | tf_op jit(solution)/shard_map/reduce_scatter | solution.py:34
  33.9 4.1 fusion.46
  38.0 0.0 all-gather.5.cloned.1.call-update
  38.1 0.0 reduce-scatter.8.cloned.1.call-start
  38.1 27.3 %all-gather.7.cloned.1.call-done = bf16[2048,256]{1,0:T(8,128)(2,1)} async-done(((bf16[512,256]{1,0:T(8,128)(2,1)}), bf16[2048,256]{1,0:T(8,128)(2,1)}) %all-gather.7.cloned.1.call-update) | async-done | bytes 1048592 | tf_op jit(solution)/shard_map/all_gather | solution.py:45
  65.4 2.1 convolution_convert_fusion
  67.4 80.1 %all-gather.5.cloned.1.call-done = bf16[2048,1024]{1,0:T(8,128)(2,1)} async-done(((bf16[512,1024]{1,0:T(8,128)(2,1)}), bf16[2048,1024]{1,0:T(8,128)(2,1)}) %all-gather.5.cloned.1.call-update) | async-done | bytes 4194320 | tf_op jit(solution)/shard_map/all_gather | solution.py:45
  147.5 4.9 %convolution_convert_fusion.1 = bf16[512,2048]{1,0:T(8,128)(2,1)S(1)} fusion(bf16[512,1024]{1,0:T(8,128)(2,1)} %get-tuple-element.8, bf16[2048,1024]{1,0:T(8,128)(2,1)} %all-gather.5.cloned.1.call-done), kind=kOutput, calls=%fused_computation.11 | convolution fusion | flops 2148532224 | bytes 7340032 | tf_op jit(solution)/shard_map/dot_general | solution.py:28
  152.4 2.5 pad_maximum_fusion
  154.9 0.0 reduce-scatter.8.cloned.1.call-update
  154.9 0.0 all-gather.9.cloned.1.call-start
  154.9 49.8 %reduce-scatter.8.cloned.1.call-done = bf16[128,2048]{1,0:T(8,128)(2,1)} async-done(((bf16[1024,2048]{1,0:T(8,128)(2,1)}), bf16[128,2048]{1,0:T(8,128)(2,1)}) %reduce-scatter.8.cloned.1.call-update) | async-done | bytes 524304 | tf_op jit(solution)/shard_map/reduce_scatter | solution.py:49
  204.7 0.0 all-gather.9.cloned.1.call-update
  204.7 0.0 all-gather.11.cloned.1.call-start
  204.8 0.5 iota_add_fusion
  205.3 114.4 %all-gather.9.cloned.1.call-done = bf16[2048,2048]{1,0:T(8,128)(2,1)} async-done(((bf16[128,2048]{1,0:T(8,128)(2,1)}), bf16[2048,2048]{1,0:T(8,128)(2,1)}) %all-gather.9.cloned.1.call-update) | async-done | bytes 8388624 | tf_op jit(solution)/shard_map/all_gather | solution.py:56
  319.7 8.3 %fusion = f32[]{:T(128)} fusion(bf16[2048,2048]{1,0:T(8,128)(2,1)} %all-gather.9.cloned.1.call-done), kind=kLoop, calls=%fused_computation.3 | loop fusion | flops 12582911 | bytes 8388612 | tf_op jit(solution)/shard_map/reduce_sum | solution.py:63
  328.8 25.4 %fusion.2 = bf16[2048,2048]{1,0:T(8,128)(2,1)S(1)} fusion(bf16[2048,2048]{1,0:T(8,128)(2,1)} %all-gather.9.cloned.1.call-done, f32[]{:T(128)S(6)} %mul.167, f32[]{:T(128)S(6)} %mul.163), kind=kOutput, calls=%fused_computation.5 | convolution fusion | flops 17200840704 | bytes 16777224 | tf_op jit(solution)/shard_map/dot_general | solution.py:19
  354.2 19.7 %fusion.4 = bf16[2048,2048]{1,0:T(8,128)(2,1)} fusion(bf16[2048,2048]{1,0:T(8,128)(2,1)S(1)} %copy-done.3, bf16[2048,2048]{1,0:T(8,128)(2,1)S(1)} %fusion.2, f32[]{:T(128)S(6)} %div.3, f32[]{:T(128)S(6)} %mul.174), kind=kOutput, calls=%fused_computation.7 | convolution fusion | flops 17200840704 | bytes 25165832 | tf_op jit(solution)/shard_map/dot_general | solution.py:19
  373.9 22.5 %add_convert_fusion = bf16[2048,2048]{1,0:T(8,128)(2,1)S(1)} fusion(bf16[2048,2048]{1,0:T(8,128)(2,1)} %fusion.4, bf16[2048,2048]{1,0:T(8,128)(2,1)S(1)} %fusion.2), kind=kOutput, calls=%fused_computation.8 | convolution fusion | flops 17196646400 | bytes 25165824 | tf_op jit(solution)/shard_map/dot_general | solution.py:19
  396.4 1.4 fusion.7
  397.9 1.4 convolution_add_fusion.1
  399.3 1.3 fusion.34
  400.6 1.6 fusion.8
  402.2 2.3 fusion.31
  404.5 9.0 %fusion.21 = f32[128,2048]{1,0:T(8,128)S(1)} fusion(bf16[2048,2048]{1,0:T(8,128)(2,1)} %copy-done, f32[128,2048]{1,0:T(8,128)} %fusion.31, f32[128,2048]{1,0:T(8,128)S(1)} %fusion.8), kind=kOutput, calls=%fused_computation.41 | convolution fusion | flops 2149318656 | bytes 11534336 | tf_op jit(solution)/shard_map/dot_general | solution.py:19
  413.5 4.8 fusion.27
  418.3 1.0 copy-done.1
  419.2 1.7 fusion.12
  420.9 0.0 slice-start
  420.9 1.5 fusion.24
  422.4 0.0 copy-start.5
  422.4 1.6 fusion.14
  424.0 0.7 slice-done.1
  424.8 2.4 fusion.15
  427.2 0.0 all-gather.11.cloned.1.call-update
  427.2 34.9 %all-gather.11.cloned.1.call-done = bf16[1024,2048]{1,0:T(8,128)(2,1)} async-done(((bf16[128,2048]{1,0:T(8,128)(2,1)}), bf16[1024,2048]{1,0:T(8,128)(2,1)}) %all-gather.11.cloned.1.call-update) | async-done | bytes 4194320 | tf_op jit(solution)/shard_map/all_gather | solution.py:87
  462.1 7.4 %broadcast_multiply_fusion = (f32[512,1024]{1,0:T(8,128)}, f32[512,1024]{1,0:T(8,128)}) fusion(f32[512,1024]{1,0:T(8,128)S(1)} %copy-done.7, bf16[2048,1024]{1,0:T(8,128)(2,1)} %all-gather.5.cloned.1.call-done, bf16[1024,2048]{1,0:T(8,128)(2,1)} %all-gather.11.cloned.1.call-done), kind=kOutput, calls=%fused_computation.39 | convolution fusion | flops 2149056512 | bytes 12582912 | tf_op jit(solution)/shard_map/dot_general | solution.py:19
  469.6 1.7 broadcast_multiply_fusion.1
  (19 shorter events, 0.0 us)
Async XLA Ops:
  7.2 13.7 %reduce-scatter.6.cloned.1.call-start = ((), (), s32[]{:S(2)}) async-start(), calls=%async_computation.5 | async-start | bytes 786432 | tf_op jit(solution)/shard_map/reduce_scatter | solution.py:34
  7.9 26.0 %reduce-scatter.4.cloned.1.call-start = ((), (), s32[]{:S(2)}) async-start(), calls=%async_computation.3 | async-start | bytes 3145728 | tf_op jit(solution)/shard_map/reduce_scatter | solution.py:34
  8.7 56.7 %all-gather.7.cloned.1.call-start = ((), (), s32[]{:S(2)}) async-start(), calls=%async_computation.6 | async-start | bytes 1310720 | tf_op jit(solution)/shard_map/all_gather | solution.py:45
  23.0 124.5 %all-gather.5.cloned.1.call-start = ((), (), s32[]{:S(2)}) async-start(), calls=%async_computation.4 | async-start | bytes 5242880 | tf_op jit(solution)/shard_map/all_gather | solution.py:45
  38.1 166.6 %reduce-scatter.8.cloned.1.call-start = ((), (), s32[]{:S(2)}) async-start(), calls=%async_computation.7 | async-start | bytes 4718592 | tf_op jit(solution)/shard_map/reduce_scatter | solution.py:49
  154.9 164.8 %all-gather.9.cloned.1.call-start = ((), (), s32[]{:S(2)}) async-start(), calls=%async_computation.8 | async-start | bytes 8912896 | tf_op jit(solution)/shard_map/all_gather | solution.py:56
  204.7 257.4 %all-gather.11.cloned.1.call-start = ((), (), s32[]{:S(2)}) async-start(), calls=%async_computation.9 | async-start | bytes 4718592 | tf_op jit(solution)/shard_map/all_gather | solution.py:87
  328.8 25.4 %copy-start.3 = (bf16[2048,2048]{1,0:T(8,128)(2,1)S(1)}, bf16[2048,2048]{1,0:T(8,128)(2,1)}, u32[]{:S(2)}) copy-start(bf16[2048,2048]{1,0:T(8,128)(2,1)} %all-gather.9.cloned.1.call-done) | copy-start | bytes 25165828
  354.2 19.8 %copy-start.2 = (bf16[2048,2048]{1,0:T(8,128)(2,1)}, bf16[2048,2048]{1,0:T(8,128)(2,1)S(1)}, u32[]{:S(2)}) copy-start(bf16[2048,2048]{1,0:T(8,128)(2,1)S(1)} %fusion.2) | copy-start | bytes 25165828
  396.4 5.7 %copy-start = (bf16[2048,2048]{1,0:T(8,128)(2,1)}, bf16[2048,2048]{1,0:T(8,128)(2,1)S(1)}, u32[]{:S(2)}) copy-start(bf16[2048,2048]{1,0:T(8,128)(2,1)S(1)} %add_convert_fusion) | copy-start | bytes 25165828
  413.5 5.8 %copy-start.1 = (bf16[2048,2048]{1,0:T(8,128)(2,1)S(1)}, bf16[2048,2048]{1,0:T(8,128)(2,1)}, u32[]{:S(2)}) copy-start(bf16[2048,2048]{1,0:T(8,128)(2,1)} %copy-done) | copy-start | bytes 25165828
  420.9 3.1 slice-start
  422.4 2.4 slice-start.1
  422.4 2.4 copy-start.5
  424.7 37.4 %copy-start.7 = (f32[512,1024]{1,0:T(8,128)S(1)}, f32[512,1024]{1,0:T(8,128)}, u32[]{:S(2)}) copy-start(f32[512,1024]{1,0:T(8,128)} %param.6) | copy-start | bytes 6291460
  427.2 42.4 %copy-start.4 = (bf16[2048,256]{1,0:T(8,128)(2,1)S(1)}, bf16[2048,256]{1,0:T(8,128)(2,1)}, u32[]{:S(2)}) copy-start(bf16[2048,256]{1,0:T(8,128)(2,1)} %all-gather.7.cloned.1.call-done) | copy-start | bytes 3145732
  462.1 7.4 %copy-start.6 = (bf16[1024,2048]{1,0:T(8,128)(2,1)S(1)}, bf16[1024,2048]{1,0:T(8,128)(2,1)}, u32[]{:S(2)}) copy-start(bf16[1024,2048]{1,0:T(8,128)(2,1)} %all-gather.11.cloned.1.call-done) | copy-start | bytes 12582916
  462.1 7.4 %copy-start.8 = (f32[512,256]{1,0:T(8,128)S(1)}, f32[512,256]{1,0:T(8,128)}, u32[]{:S(2)}) copy-start(f32[512,256]{1,0:T(8,128)} %param.9) | copy-start | bytes 1572868
Sparse Core Ops, SparseCore 0:
  10.2 10.6 reduce-scatter.5
  23.1 10.7 reduce-scatter.3
  36.1 29.2 all-gather.6
  67.4 80.1 all-gather.4
  155.0 49.6 reduce-scatter.7
  207.3 112.2 all-gather.8
  427.3 34.7 all-gather.10
